TPU v7x, 256 devices: a whole 4x4x8 slice. The times are simulated.
256 devices in a mesh: sp: 16 (over y, x), tp: 16 (over z, core).
Axes of the slice: x: 4, y: 4, z: 8, core: 2. Of those that a mesh axis runs over, the one named last changes fastest.
Arguments:
- residual: bfloat16 [8192, 2048], P(('sp', 'tp')), may hold values from -6 to 6
- queries: bfloat16 [8192, 4096], P('sp', 'tp'), may hold values from -6 to 6
- keys: bfloat16 [8192, 4096], P('sp', 'tp'), may hold values from -6 to 6
- values: bfloat16 [8192, 4096], P('sp', 'tp'), may hold values from -6 to 6
- in_gate: float32 [16, 8192], P('tp', 'sp'), may hold values from -5 to 130
- forget_gate: float32 [16, 8192], P('tp', 'sp'), may hold values from 0 to 16
- doc_ids: int32 [8192], P('sp'), may hold values from 0 to 7, never falling along the last dimension, each value on 1 to 4096 neighbouring positions
- head_gain: float32 [4096], P('tp'), may hold values from 0.1 to 1.9
- out_weight: bfloat16 [4096, 2048], P('tp'), may hold values from -0.09375 to 0.09375
- norm_gain: float32 [2048], replicated, may hold values from 0.1 to 1.9
- route_ids: int32 [8192, 2], P(('sp', 'tp')), may hold values from 0 to 15, all different within a row; in each aligned block of 32 rows (0 to 31, 32 to 63, ...) at most 5 rows name the same one
- route_weights: float32 [8192, 2], P(('sp', 'tp')), may hold values from 0.2 to 1
- gate_proj: bfloat16 [16, 2048, 4096], P('sp', None, 'tp'), may hold values from -0.125 to 0.125
- up_proj: bfloat16 [16, 2048, 4096], P('sp', None, 'tp'), may hold values from -0.125 to 0.125
- down_proj: bfloat16 [16, 4096, 2048], P('sp', 'tp'), may hold values from -0.09375 to 0.09375
Outputs:
- mixed: bfloat16 [8192, 2048], P(('sp', 'tp'))
Inputs may be any that keep to these rules, and one draw needn't show every extreme that they name: `route_ids`: each row names 2 different experts. In each aligned block of 32 rows (the rows of one device) no expert is named by more than 5 rows, and in some blocks one expert by exactly 5. `doc_ids`: numbers never fall along the sequence; no document covers more than half of the 8192 positions, and one covers exactly half.
All inputs are finite; a program needn't handle non-finite values.
Results may differ from a plain program's by a relative error of at most 0.018.
Values may be sent and summed in bfloat16 or wider, within the bound.
A program may use at most 64 MiB of HBM per device.

v0:
```python
import math
import jax
import jax.numpy as jnp
from jax import lax
from jax.sharding import Mesh
from jax.sharding import PartitionSpec as P

SP = ("sp_0", "sp_1")
SP_TP = ("sp_0", "sp_1", "tp")
MASKED = -1e30
EPSILON = 1e-06


def neutral_like(value, identity):
    return jax.tree.map(
        lambda a, e: jnp.broadcast_to(jnp.asarray(e, a.dtype), a.shape), value, identity
    )


def carried_in(value, axes, combine, identity):
    before = start = neutral_like(value, identity)
    running = value
    for axis in reversed(axes):
        peers, index = (lax.axis_size(axis), lax.axis_index(axis))
        pieces = jax.tree.map(lambda part: lax.all_gather(part, axis), running)
        inside, running = (start, start)
        for k in range(peers):
            passed = k < index
            running = combine(running, jax.tree.map(lambda part: part[k], pieces))
            inside = jax.tree.map(lambda new, old: jnp.where(passed, new, old), running, inside)
        before = combine(inside, before)
    return before


def block_step(state, pieces):
    memory, normalizer, max_level, carry_doc = state
    q_block, k_block, v_block, in_block, forget_block, doc_block = pieces
    scaling = q_block.shape[1] ** (-0.5)
    cum_forget = jnp.cumsum(forget_block)
    positions = jnp.arange(q_block.shape[0])
    permitted_mask = (positions[:, None] >= positions[None, :]) & (
        doc_block[:, None] == doc_block[None, :]
    )
    log_weights = jnp.where(
        permitted_mask, cum_forget[:, None] - cum_forget[None, :] + in_block[None, :], MASKED
    )
    carried = jnp.where(doc_block == carry_doc, cum_forget + max_level, MASKED)
    row_max = jnp.maximum(carried, jnp.max(log_weights, axis=1))
    scores = jnp.dot(q_block, k_block.T, preferred_element_type=jnp.float32) * scaling
    weighted = scores * jnp.exp(log_weights - row_max[:, None])
    carry_weight = jnp.exp(carried - row_max)
    query_scaled = q_block.astype(jnp.float32) * scaling
    key_full = k_block.astype(jnp.float32)
    value_full = v_block.astype(jnp.float32)
    readout_numerator = jnp.dot(weighted, value_full, precision=lax.Precision.HIGHEST)
    readout_numerator = readout_numerator + carry_weight[:, None] * jnp.dot(
        query_scaled, memory.T, precision=lax.Precision.HIGHEST
    )
    denominator = jnp.sum(weighted, axis=1) + carry_weight * jnp.dot(
        query_scaled, normalizer, precision=lax.Precision.HIGHEST
    )
    last_doc = doc_block[-1]
    forget_total = cum_forget[-1]
    log_end = jnp.where(doc_block == last_doc, forget_total - cum_forget + in_block, MASKED)
    carry_log = jnp.where(carry_doc == last_doc, forget_total + max_level, MASKED)
    new_max = jnp.maximum(carry_log, jnp.max(log_end))
    end_weight = jnp.exp(log_end - new_max)
    kept_share = jnp.exp(carry_log - new_max)
    new_memory = kept_share * memory + jnp.dot(
        (value_full * end_weight[:, None]).T, key_full, precision=lax.Precision.HIGHEST
    )
    new_normalizer = kept_share * normalizer + jnp.dot(
        end_weight, key_full, precision=lax.Precision.HIGHEST
    )
    return (
        (new_memory, new_normalizer, new_max, last_doc),
        (readout_numerator, denominator, row_max),
    )


def run_blocks(
    queries_in,
    keys_in,
    incoming_vectors,
    in_gates,
    log_forget,
    doc_row,
    memory,
    normalizer,
    max_level,
    carry_doc,
):
    extent = queries_in.shape[0]
    block_size = math.gcd(extent, 256)
    blocks = extent // block_size

    def to_blocks(tensor):
        return tensor.reshape((blocks, block_size) + tensor.shape[1:])

    pieces = tuple(
        (
            to_blocks(tensor)
            for tensor in (queries_in, keys_in, incoming_vectors, in_gates, log_forget, doc_row)
        )
    )
    final_state, outputs = lax.scan(block_step, (memory, normalizer, max_level, carry_doc), pieces)
    readout_numerator, denominator, row_max = outputs
    return (
        readout_numerator.reshape(extent, -1),
        denominator.reshape(extent),
        row_max.reshape(extent),
        final_state,
    )


def combine_states(earlier, later):
    memory_a, normal_a, level_a, forget_a, first_a, last_a = earlier
    memory_b, normal_b, level_b, forget_b, first_b, last_b = later
    joined = (last_a == first_b) | (last_a < 0) | (first_b < 0)
    passed = forget_b + jnp.where(joined, 0.0, MASKED)
    new_level = jnp.maximum(passed + level_a, level_b)
    share_a = jnp.exp(passed + level_a - new_level)
    fraction_second = jnp.exp(level_b - new_level)
    new_memory = share_a[:, None, None] * memory_a + fraction_second[:, None, None] * memory_b
    new_normal = share_a[:, None] * normal_a + fraction_second[:, None] * normal_b
    first_doc = jnp.where(first_a < 0, first_b, first_a)
    last_doc = jnp.where(last_b < 0, last_a, last_b)
    return (new_memory, new_normal, new_level, forget_a + passed, first_doc, last_doc)


def on_device(
    residual,
    queries,
    keys,
    values,
    in_gate,
    forget_gate,
    doc_ids,
    head_gain,
    out_weight,
    norm_gain,
    route_ids,
    route_weights,
    gate_proj,
    up_proj,
    down_proj,
):
    extent, local_width = queries.shape
    heads_here = in_gate.shape[0]
    head_size = local_width // heads_here

    def by_head(tensor):
        return tensor.reshape(extent, heads_here, head_size).transpose(1, 0, 2)

    query_heads = by_head(queries)
    key_heads = by_head(keys)
    value_heads = by_head(values)
    log_forget = jax.nn.log_sigmoid(forget_gate)
    cum_forget = jnp.cumsum(log_forget, axis=1)
    first_doc = doc_ids[0]
    last_doc = doc_ids[-1]
    run_heads = jax.vmap(run_blocks, in_axes=(0, 0, 0, 0, 0, None, 0, 0, 0, None))
    forget_total = jnp.where(first_doc == last_doc, cum_forget[:, -1], MASKED)
    doc_first = first_doc.astype(jnp.float32).reshape(1)
    doc_last = last_doc.astype(jnp.float32).reshape(1)
    empty_memory = jnp.zeros((heads_here, head_size, head_size), jnp.float32)
    empty_normal = jnp.zeros((heads_here, head_size), jnp.float32)
    empty_level = jnp.full((heads_here,), MASKED, jnp.float32)
    identity = (
        empty_memory,
        empty_normal,
        empty_level,
        jnp.zeros((heads_here,), jnp.float32),
        jnp.full((1,), -1.0, jnp.float32),
        jnp.full((1,), -1.0, jnp.float32),
    )
    readout_numerator, denominator, row_max, final_state = run_heads(
        query_heads,
        key_heads,
        value_heads,
        in_gate,
        log_forget,
        doc_ids,
        empty_memory,
        empty_normal,
        empty_level,
        first_doc,
    )
    local_state = (
        final_state[0],
        final_state[1],
        final_state[2],
        forget_total,
        doc_first,
        doc_last,
    )
    incoming = carried_in(local_state, SP, combine_states, identity)
    linked = incoming[5][0] == doc_first[0]
    in_level = jnp.where(linked, incoming[2], MASKED)
    carried = jnp.where(doc_ids[None, :] == first_doc, cum_forget + in_level[:, None], MASKED)
    new_max = jnp.maximum(row_max, carried)
    own_share = jnp.exp(row_max - new_max)
    far_share = jnp.exp(carried - new_max)
    query_scaled = query_heads.astype(jnp.float32) * head_size ** (-0.5)
    readout_numerator = own_share[..., None] * readout_numerator + far_share[
        ..., None
    ] * jnp.einsum("htd,hvd->htv", query_scaled, incoming[0], precision=lax.Precision.HIGHEST)
    denominator = own_share * denominator + far_share * jnp.einsum(
        "htd,hd->ht", query_scaled, incoming[1], precision=lax.Precision.HIGHEST
    )
    mixed_heads = (
        readout_numerator / jnp.maximum(jnp.abs(denominator), jnp.exp(-new_max))[..., None]
    )
    normed_heads = mixed_heads * lax.rsqrt(
        jnp.mean(mixed_heads * mixed_heads, axis=-1, keepdims=True) + EPSILON
    )
    normed_heads = normed_heads * head_gain.reshape(heads_here, 1, head_size)
    head_rows = normed_heads.transpose(1, 0, 2).reshape(extent, local_width).astype(jnp.bfloat16)
    rows_here, model_width = residual.shape
    update = lax.psum_scatter(
        jnp.dot(head_rows, out_weight, preferred_element_type=jnp.float32).astype(jnp.bfloat16),
        "tp",
        scatter_dimension=0,
        tiled=True,
    ).astype(jnp.float32)
    stream = residual.astype(jnp.float32) + update
    normed = (
        stream * lax.rsqrt(jnp.mean(stream * stream, axis=-1, keepdims=True) + EPSILON) * norm_gain
    )
    normed = normed.astype(jnp.bfloat16)
    experts_all = gate_proj.shape[0] * lax.axis_size(SP)
    top_count = route_ids.shape[1]
    capacity = max(2, rows_here * top_count * 5 // (4 * experts_all))
    flat_ids = route_ids.reshape(-1)
    onehot = (flat_ids[:, None] == jnp.arange(experts_all, dtype=jnp.int32)[None, :]).astype(
        jnp.int32
    )
    earlier = jnp.cumsum(onehot, axis=0) - onehot
    slot_rank = jnp.sum(earlier * onehot, axis=1)
    slot_index = flat_ids * capacity + slot_rank
    placing = (
        slot_index[None, :] == jnp.arange(experts_all * capacity, dtype=jnp.int32)[:, None]
    ).astype(jnp.bfloat16)
    copies = jnp.repeat(normed, top_count, axis=0)
    outgoing = jnp.dot(placing, copies, preferred_element_type=jnp.float32).astype(jnp.bfloat16)
    outgoing = outgoing.reshape(experts_all, capacity, model_width)
    arrived = lax.all_to_all(outgoing, SP, split_axis=0, concat_axis=0, tiled=True).reshape(
        -1, model_width
    )
    piece = lax.all_gather(arrived, "tp", axis=0, tiled=True)
    gate_part = jnp.dot(piece, gate_proj[0], preferred_element_type=jnp.float32)
    up_part = jnp.dot(piece, up_proj[0], preferred_element_type=jnp.float32)
    hidden = (jax.nn.silu(gate_part) * up_part).astype(jnp.bfloat16)
    expert_sum = lax.psum_scatter(
        jnp.dot(hidden, down_proj[0], preferred_element_type=jnp.float32).astype(jnp.bfloat16),
        "tp",
        scatter_dimension=0,
        tiled=True,
    )
    expert_out = expert_sum.reshape(experts_all, capacity, model_width)
    returned = lax.all_to_all(expert_out, SP, split_axis=0, concat_axis=0, tiled=True)
    picked = jnp.take(returned.reshape(-1, model_width), slot_index, axis=0)
    picked = picked.reshape(rows_here, top_count, model_width)
    expert_mix = jnp.sum(route_weights[..., None] * picked.astype(jnp.float32), axis=1)
    return (stream + expert_mix).astype(jnp.bfloat16)


def solution(mesh):
    finer = Mesh(mesh.devices.reshape(4, 4, mesh.shape["tp"]), ("sp_0", "sp_1", "tp"))
    in_specs = (
        P(SP_TP, None),
        P(SP, "tp"),
        P(SP, "tp"),
        P(SP, "tp"),
        P("tp", SP),
        P("tp", SP),
        P(SP),
        P("tp"),
        P("tp", None),
        P(),
        P(SP_TP, None),
        P(SP_TP, None),
        P(SP, None, "tp"),
        P(SP, None, "tp"),
        P(SP, "tp", None),
    )
    out_specs = P(SP_TP, None)
    return jax.shard_map(
        on_device, mesh=finer, in_specs=in_specs, out_specs=out_specs, check_vma=False
    )
```

profile of v0, /device:TPU:2, one launch (start us, length us, event | category | flops | bytes accessed | tf_op | source)
XLA Modules:
  0.0 372.2 jit_solution(4518122679349654062)
XLA Ops:
  6.5 1.4 fusion.182
  10.0 25.1 %while.23 = (s32[]{:T(128)}, f32[1,256,256]{2,1,0:T(8,128)S(1)}, f32[1,256]{1,0:T(1,128)S(1)}, f32[1]{0:T(128)}, s32[]{:T(128)}, /*index=5*/f32[2,1,256,256]{3,2...) while((s32[]{:T(128)}, f32[1,256,256]{2,1,0:T(8,128)S(1)}, ...), condition=%wide.region_6.7_spmd.clone, body=%wide.region_0.6_spmd.clone.sunk | while | flops 641046528 | bytes 6349332 | solution.py:106
  13.2 1.3 fusion.226
  15.7 1.9 fusion.223
  17.6 1.3 fusion.227
  24.5 1.2 fusion.225
  25.7 1.3 fusion.226
  28.2 1.9 fusion.223
  30.1 1.3 fusion.227
  45.2 10.0 %all-reduce.8 = (f32[4]{0:T(128)S(1)}, f32[4]{0:T(128)S(1)}, f32[4]{0:T(128)S(1)}, f32[4]{0:T(128)S(1)}) all-reduce(f32[4]{0:T(128)S(1)} %dynamic-update-slice, f32[4]{0:T(128)S(1)} %fusion.156, f32[4]{0:T(128)S(1)} %dynamic-update-slice.3, f32[4]{0:T(128)S(1)} %dynamic-update-slice.6), channel_id=1, replica_groups=mesh['sp_0'=4,'sp_1'=4,'tp'=16] {'sp_1'}, use_global_device_ids=true, to_apply=%add | all-reduce | flops 16 | bytes 128
  55.9 2.6 fusion.152
  65.8 1.2 fusion.189
  72.3 2.0 fusion.70
  75.1 1.9 fusion.188
  78.2 1.4 dynamic-update-slice.7
  80.3 1.4 dynamic-update-slice.5
  81.8 1.4 dynamic-update-slice.1
  83.2 9.3 %all-reduce.9 = (f32[4]{0:T(128)S(1)}, f32[4]{0:T(128)S(1)}, f32[4]{0:T(128)S(1)}, f32[4]{0:T(128)S(1)}) all-reduce(f32[4]{0:T(128)S(1)} %dynamic-update-slice.1, f32[4]{0:T(128)S(1)} %dynamic-update-slice.4, f32[4]{0:T(128)S(1)} %dynamic-update-slice.5, f32[4]{0:T(128)S(1)} %dynamic-update-slice.7), channel_id=2, replica_groups=mesh['sp_0'=4,'sp_1'=4,'tp'=16] {'sp_0'}, use_global_device_ids=true, to_apply=%add.1 | all-reduce | flops 16 | bytes 128
  121.3 9.6 %all-gather.8 = f32[4,1,256]{2,1,0:T(1,128)S(1)} all-gather(f32[1,1,256]{2,1,0:T(1,128)S(1)} %bitcast.322), channel_id=9, replica_groups=mesh['sp_0'=4,'sp_1'=4,'tp'=16] {'sp_1'}, dimensions={0}, use_global_device_ids=true | all-gather | bytes 5120 | tf_op jit(solution)/shard_map/all_gather | solution.py:25
  130.9 7.0 %all_gather.84 = f32[4,1,256]{2,1,0:T(1,128)S(1)} all-gather(f32[1,1,256]{2,1,0:T(1,128)S(1)} %get-tuple-element.176), channel_id=1, replica_groups=mesh['sp_0'=4,'sp_1'=4,'tp'=16] {'sp_0'}, dimensions={0}, use_global_device_ids=true | all-gather | bytes 5120 | tf_op jit(solution)/shard_map/all_gather | solution.py:25
  139.3 2.6 multiply_reduce_fusion.1
  141.9 2.2 convolution_convert_fusion.1
  144.7 59.9 %reduce-scatter.3.cloned.1.call-done = bf16[32,2048]{1,0:T(8,128)(2,1)} async-done(((bf16[512,2048]{1,0:T(8,128)(2,1)}), bf16[32,2048]{1,0:T(8,128)(2,1)}) %reduce-scatter.3.cloned.1.call-update) | async-done | bytes 131088 | tf_op jit(solution)/shard_map/reduce_scatter | solution.py:220
  207.4 15.9 %all_to_all.10 = bf16[16,5,2048]{2,1,0:T(8,128)(2,1)S(1)} all-to-all(bf16[16,5,2048]{2,1,0:T(8,128)(2,1)S(1)} %reshape.898), channel_id=1, replica_groups=mesh['sp_0'=4,'sp_1'=4,'tp'=16] {'sp_0','sp_1'}, dimensions={0} | all-to-all | bytes 655360 | tf_op jit(solution)/shard_map/all_to_all | solution.py:247
  224.4 40.1 %all-gather.15.cloned.1.call-done = bf16[1280,2048]{1,0:T(8,128)(2,1)} async-done(((bf16[80,2048]{1,0:T(8,128)(2,1)}), bf16[1280,2048]{1,0:T(8,128)(2,1)}) %all-gather.15.cloned.1.call-update) | async-done | bytes 5242896 | tf_op jit(solution)/shard_map/all_gather | solution.py:250
  264.5 5.1 %fusion.56 = f32[1280,256]{1,0:T(8,128)} fusion(bf16[1280,2048]{1,0:T(8,128)(2,1)} %all-gather.15.cloned.1.call-done, bf16[1,2048,256]{2,1,0:T(8,128)(2,1)S(1)} %copy-done.14), kind=kOutput, calls=%fused_computation.85 | convolution fusion | flops 1342177280 | bytes 7602176 | tf_op jit(solution)/shard_map/dot_general | solution.py:251
  269.6 10.6 %convolution_convert_fusion = bf16[1280,2048]{1,0:T(8,128)(2,1)} fusion(bf16[1280,2048]{1,0:T(8,128)(2,1)} %all-gather.15.cloned.1.call-done, f32[1280,256]{1,0:T(8,128)} %fusion.56, bf16[1,256,2048]{2,1,0:T(8,128)(2,1)S(1)} %copy-done, bf16[1,2048,256]{2,1,0:T(8,128)(2,1)S(1)} %copy-done.15), kind=kOutput, calls=%fused_computation.75 | convolution fusion | flops 2688942080 | bytes 13893632 | tf_op jit(solution)/shard_map/dot_general | solution.py:255
  280.9 63.2 %reduce-scatter.5.cloned.1.call-done = bf16[80,2048]{1,0:T(8,128)(2,1)} async-done(((bf16[1280,2048]{1,0:T(8,128)(2,1)}), bf16[80,2048]{1,0:T(8,128)(2,1)}) %reduce-scatter.5.cloned.1.call-update) | async-done | bytes 327696 | tf_op jit(solution)/shard_map/reduce_scatter | solution.py:254
  344.2 1.9 reshape.900
  346.1 7.3 %all-to-all-start.1 = ((bf16[16,5,2048]{2,1,0:T(8,128)(2,1)}), bf16[16,5,2048]{2,1,0:T(8,128)(2,1)S(1)}, u32[]{:S(2)}, u32[]{:S(2)}) async-start(bf16[16,5,2048]{2,1,0:T(8,128)(2,1)} %reshape.900), calls=%async_computation.3 | async-start | bytes 1048576 | tf_op jit(solution)/shard_map/all_to_all | solution.py:261
  353.4 8.7 %all-to-all-done.1 = bf16[16,5,2048]{2,1,0:T(8,128)(2,1)S(1)} async-done(((bf16[16,5,2048]{2,1,0:T(8,128)(2,1)}), bf16[16,5,2048]{2,1,0:T(8,128)(2,1)S(1)}, u32[]{:S(2)}, u32[]{:S(2)}) %all-to-all-start.1) | async-done | bytes 327712 | tf_op jit(solution)/shard_map/all_to_all | solution.py:261
  363.2 1.8 multiply_reduce_fusion
  (161 shorter events, 32.4 us)
Async XLA Ops:
  6.5 263.0 %copy-start = (bf16[1,256,2048]{2,1,0:T(8,128)(2,1)S(1)}, bf16[1,256,2048]{2,1,0:T(8,128)(2,1)}, u32[]{:S(2)}) copy-start(bf16[1,256,2048]{2,1,0:T(8,128)(2,1)} %param.31) | copy-start | bytes 3145732
  6.5 65.7 %all-gather.17.cloned.1.call-start = ((), (), s32[]{:S(2)}) async-start(), calls=%async_computation.8 | async-start | bytes 1310720 | tf_op jit(solution)/shard_map/all_gather | solution.py:25
  10.0 31.6 %copy-start.17 = (u32[256]{0:T(256)S(1)}, u32[256]{0:T(256)}, u32[]{:S(2)}) copy-start(u32[256]{0:T(256)} %constant.127) | copy-start | bytes 3076
  10.0 64.3 %copy-start.16 = (u32[256]{0:T(256)S(1)}, u32[256]{0:T(256)}, u32[]{:S(2)}) copy-start(u32[256]{0:T(256)} %constant.132) | copy-start | bytes 3076
  10.1 10.8 %copy-start.4 = (bf16[2,1,256,256]{3,2,1,0:T(8,128)(2,1)S(1)}, bf16[2,1,256,256]{3,2,1,0:T(8,128)(2,1)}, u32[]{:S(2)}) copy-start(bf16[2,1,256,256]{3,2,1,0:T(8,128)(2,1)} %get-tuple-element.388) | copy-start | bytes 786436 | tf_op jit(solution)/shard_map/vmap()/while
  10.1 10.8 %copy-start.5 = (bf16[2,1,256,256]{3,2,1,0:T(8,128)(2,1)S(1)}, bf16[2,1,256,256]{3,2,1,0:T(8,128)(2,1)}, u32[]{:S(2)}) copy-start(bf16[2,1,256,256]{3,2,1,0:T(8,128)(2,1)} %get-tuple-element.387) | copy-start | bytes 786436 | tf_op jit(solution)/shard_map/vmap()/while
  10.1 11.3 %copy-start.2 = (bf16[2,1,256,256]{3,2,1,0:T(8,128)(2,1)S(1)}, bf16[2,1,256,256]{3,2,1,0:T(8,128)(2,1)}, u32[]{:S(2)}) copy-start(bf16[2,1,256,256]{3,2,1,0:T(8,128)(2,1)} %get-tuple-element.389) | copy-start | bytes 786436 | tf_op jit(solution)/shard_map/vmap()/while
  22.6 10.8 %copy-start.4 = (bf16[2,1,256,256]{3,2,1,0:T(8,128)(2,1)S(1)}, bf16[2,1,256,256]{3,2,1,0:T(8,128)(2,1)}, u32[]{:S(2)}) copy-start(bf16[2,1,256,256]{3,2,1,0:T(8,128)(2,1)} %get-tuple-element.388) | copy-start | bytes 786436 | tf_op jit(solution)/shard_map/vmap()/while
  22.6 10.8 %copy-start.5 = (bf16[2,1,256,256]{3,2,1,0:T(8,128)(2,1)S(1)}, bf16[2,1,256,256]{3,2,1,0:T(8,128)(2,1)}, u32[]{:S(2)}) copy-start(bf16[2,1,256,256]{3,2,1,0:T(8,128)(2,1)} %get-tuple-element.387) | copy-start | bytes 786436 | tf_op jit(solution)/shard_map/vmap()/while
  22.6 11.3 %copy-start.2 = (bf16[2,1,256,256]{3,2,1,0:T(8,128)(2,1)S(1)}, bf16[2,1,256,256]{3,2,1,0:T(8,128)(2,1)}, u32[]{:S(2)}) copy-start(bf16[2,1,256,256]{3,2,1,0:T(8,128)(2,1)} %get-tuple-element.389) | copy-start | bytes 786436 | tf_op jit(solution)/shard_map/vmap()/while
  35.1 0.7 copy-start.1
  35.1 102.7 %copy-start.9 = (s32[512]{0:T(512)S(1)}, s32[512]{0:T(512)}, u32[]{:S(2)}) copy-start(s32[512]{0:T(512)} %param.23) | copy-start | bytes 6148
  35.2 103.5 %copy-start.3 = (bf16[2,1,256,256]{3,2,1,0:T(8,128)(2,1)S(1)}, bf16[2,1,256,256]{3,2,1,0:T(8,128)(2,1)}, u32[]{:S(2)}) copy-start(bf16[2,1,256,256]{3,2,1,0:T(8,128)(2,1)} %get-tuple-element.404) | copy-start | bytes 786436
  35.9 103.4 %all-gather.13.cloned.1.call-start = ((), (), s32[]{:S(2)}) async-start(), calls=%async_computation.4 | async-start | bytes 1310720 | tf_op jit(solution)/shard_map/all_gather | solution.py:25
  74.3 130.3 %reduce-scatter.3.cloned.1.call-start = ((), (), s32[]{:S(2)}) async-start(), calls=%async_computation.5 | async-start | bytes 2228224 | tf_op jit(solution)/shard_map/reduce_scatter | solution.py:220
  139.3 2.6 copy-start.8
  139.3 2.6 copy-start.13
  141.9 2.3 copy-start.10
  141.9 62.7 %copy-start.6 = (bf16[32,2048]{1,0:T(8,128)(2,1)S(1)}, bf16[32,2048]{1,0:T(8,128)(2,1)}, u32[]{:S(2)}) copy-start(bf16[32,2048]{1,0:T(8,128)(2,1)} %param.17) | copy-start | bytes 393220
  144.1 61.6 %copy-start.11 = (f32[2048]{0:T(1024)S(1)}, f32[2048]{0:T(1024)}, u32[]{:S(2)}) copy-start(f32[2048]{0:T(1024)} %param.26) | copy-start | bytes 24580
  144.1 120.3 %all-gather.15.cloned.1.call-start = ((), (), s32[]{:S(2)}) async-start(), calls=%async_computation.6 | async-start | bytes 5570560 | tf_op jit(solution)/shard_map/all_gather | solution.py:250
  206.9 57.6 %copy-start.14 = (bf16[1,2048,256]{2,1,0:T(8,128)(2,1)S(1)}, bf16[1,2048,256]{2,1,0:T(8,128)(2,1)}, u32[]{:S(2)}) copy-start(bf16[1,2048,256]{2,1,0:T(8,128)(2,1)} %param.29) | copy-start | bytes 3145732
  224.1 45.4 %copy-start.15 = (bf16[1,2048,256]{2,1,0:T(8,128)(2,1)S(1)}, bf16[1,2048,256]{2,1,0:T(8,128)(2,1)}, u32[]{:S(2)}) copy-start(bf16[1,2048,256]{2,1,0:T(8,128)(2,1)} %param.30) | copy-start | bytes 3145732
  224.2 120.0 %reduce-scatter.5.cloned.1.call-start = ((), (), s32[]{:S(2)}) async-start(), calls=%async_computation.7 | async-start | bytes 5570560 | tf_op jit(solution)/shard_map/reduce_scatter | solution.py:254
  280.2 0.7 copy-start.12
  346.1 16.1 %all-to-all-start.1 = ((bf16[16,5,2048]{2,1,0:T(8,128)(2,1)}), bf16[16,5,2048]{2,1,0:T(8,128)(2,1)S(1)}, u32[]{:S(2)}, u32[]{:S(2)}) async-start(bf16[16,5,2048]{2,1,0:T(8,128)(2,1)} %reshape.900), calls=%async_computation.3 | async-start | bytes 1048576 | tf_op jit(solution)/shard_map/all_to_all | solution.py:261
  353.4 11.6 %copy-start.7 = (bf16[32,2048]{1,0:T(8,128)(2,1)S(1)}, bf16[32,2048]{1,0:T(8,128)(2,1)}, u32[]{:S(2)}) copy-start(bf16[32,2048]{1,0:T(8,128)(2,1)} %reduce-scatter.3.cloned.1.call-done) | copy-start | bytes 393220
Sparse Core Ops, SparseCore 0:
  36.0 28.4 all-gather.16
  74.5 28.0 all-gather.12
  144.2 60.3 reduce-scatter.2
  224.3 40.1 all-gather.14
  280.3 63.8 reduce-scatter.4
where the time goes:
time: 374 us; the launch traced here: 372 us
  waiting for transfers between devices  172 us (46%)
  between operations  55.8 us (15%)
  blocking collectives  51.8 us (14%)
  matrix products  30.8 us (8%)
  local copies, waits for them, and re-layouts  25.3 us (7%)
  other arithmetic  23.4 us (6%)
  starting transfers between devices  7.62 us (2%)
  loops' own time  5.4 us (1%)
    reduce_scatter x1, waiting for transfers between devices, on_device(): lax.psum_scatter(jnp.dot(hidden, down_proj[0], preferred_element_type=jnp...  63.2 us
    reduce_scatter x1, waiting for transfers between devices, on_device(): lax.psum_scatter(jnp.dot(head_rows, out_weight, preferred_element_type=jn...  59.9 us
    all_gather x1, waiting for transfers between devices, on_device(): piece = lax.all_gather(arrived, 'tp', axis=0, tiled=True)  40.1 us
    unnamed x2, blocking collectives  19.3 us
    all_gather x2, blocking collectives, carried_in(): pieces = jax.tree.map(lambda part: lax.all_gather(part, axis), running)  16.6 us
    all_to_all x1, blocking collectives, on_device(): lax.all_to_all(outgoing, SP, split_axis=0, concat_axis=0, tiled=True)  15.9 us
    dot_general x1, matrix products, on_device(): jnp.dot(hidden, down_proj[0], preferred_element_type=jnp.float32)  10.6 us
    unnamed x49, local copies, waits for them, and re-layouts  9.59 us
  transfers between devices with their start and end apart: 6, of which 4 were waited for; matrix products, arithmetic and copies ran while one was open for 7% of the time, Pallas kernels for 0%

commit v1 on v0

--- a/solution.py
+++ b/solution.py
@@ -247,7 +247,16 @@
     arrived = lax.all_to_all(outgoing, SP, split_axis=0, concat_axis=0, tiled=True).reshape(
         -1, model_width
     )
-    piece = lax.all_gather(arrived, "tp", axis=0, tiled=True)
+    ways = lax.axis_size("tp")
+    up = [(d, (d + 1) % ways) for d in range(ways)]
+    down = [(d, (d - 1) % ways) for d in range(ways)]
+    earlier_2, later_2 = ([arrived], [arrived])
+    for _ in range(ways // 2):
+        earlier_2.append(lax.ppermute(earlier_2[-1], "tp", up))
+    for _ in range((ways - 1) // 2):
+        later_2.append(lax.ppermute(later_2[-1], "tp", down))
+    line = jnp.concatenate([*earlier_2[::-1], *later_2[1:]], axis=0)
+    piece = jnp.roll(line, (lax.axis_index("tp") - ways // 2) * arrived.shape[0], axis=0)
     gate_part = jnp.dot(piece, gate_proj[0], preferred_element_type=jnp.float32)
     up_part = jnp.dot(piece, up_proj[0], preferred_element_type=jnp.float32)
     hidden = (jax.nn.silu(gate_part) * up_part).astype(jnp.bfloat16)

time: 374 us -> 414 us (1.11)
  starting transfers between devices: 7.62 us -> 28.5 us
  local copies, waits for them, and re-layouts: 25.3 us -> 40.8 us
  matrix products: 30.8 us -> 35.2 us
    ppermute x0 -> x15, waiting for transfers between devices: none -> 40.2 us  [the longest x8 38.8 us: on_device(): earlier_2.append(lax.ppermute(earlier_2[-1], 'tp', up))]
    all_gather x1 -> x0, waiting for transfers between devices: 40.1 us -> none  [on_device(): piece = lax.all_gather(arrived, 'tp', axis=0, tiled=True)]
    ppermute x0 -> x15, starting transfers between devices: none -> 21.1 us  [the longest x7 21.1 us: on_device(): later_2.append(lax.ppermute(later_2[-1], 'tp', down))]
    unnamed x49 -> x94, local copies, waits for them, and re-layouts: 9.59 us -> 25.9 us
  transfers between devices with their start and end apart: 6 -> 20, of which waited for: 4 -> 13; matrix products, arithmetic and copies ran while one was open for 7% -> 8% of each run, Pallas kernels for 0% -> 0%
where the time goes in v1:
time: 414 us; the launch traced here: 412 us
  waiting for transfers between devices  170 us (41%)
  between operations  56.4 us (14%)
  blocking collectives  51.8 us (13%)
  local copies, waits for them, and re-layouts  40.8 us (10%)
  matrix products  35.2 us (9%)
  starting transfers between devices  28.5 us (7%)
  other arithmetic  23.3 us (6%)
  loops' own time  5.38 us (1%)
    reduce_scatter x1, waiting for transfers between devices, on_device(): lax.psum_scatter(jnp.dot(hidden, down_proj[0], preferred_element_type=jnp...  61.4 us
    reduce_scatter x1, waiting for transfers between devices, on_device(): lax.psum_scatter(jnp.dot(head_rows, out_weight, preferred_element_type=jn...  60 us
    ppermute x8, waiting for transfers between devices, on_device(): earlier_2.append(lax.ppermute(earlier_2[-1], 'tp', up))  38.8 us
    unnamed x94, local copies, waits for them, and re-layouts  25.9 us
    ppermute x7, starting transfers between devices, on_device(): later_2.append(lax.ppermute(later_2[-1], 'tp', down))  21.1 us
    unnamed x2, blocking collectives  19.3 us
    all_gather x2, blocking collectives, carried_in(): pieces = jax.tree.map(lambda part: lax.all_gather(part, axis), running)  16.6 us
    all_to_all x1, blocking collectives, on_device(): lax.all_to_all(outgoing, SP, split_axis=0, concat_axis=0, tiled=True)  15.8 us
  transfers between devices with their start and end apart: 20, of which 13 were waited for; matrix products, arithmetic and copies ran while one was open for 8% of the time, Pallas kernels for 0%

profile of v1, /device:TPU:2, one launch (start us, length us, event | category | flops | bytes accessed | tf_op | source)
XLA Modules:
  0.0 411.8 jit_solution(493444347262639)
XLA Ops:
  10.1 30.5 %while.23 = (s32[]{:T(128)}, f32[1,256,256]{2,1,0:T(8,128)S(1)}, f32[1,256]{1,0:T(1,128)S(1)}, f32[1]{0:T(128)}, s32[]{:T(128)}, /*index=5*/f32[2,1,256,256]{3,2...) while((s32[]{:T(128)}, f32[1,256,256]{2,1,0:T(8,128)S(1)}, ...), condition=%wide.region_6.7_spmd.clone, body=%wide.region_0.6_spmd.clone.sunk | while | flops 641046528 | bytes 3205044 | solution.py:106
  50.1 10.0 %all-reduce.8 = (f32[4]{0:T(128)S(1)}, f32[4]{0:T(128)S(1)}, f32[4]{0:T(128)S(1)}, f32[4]{0:T(128)S(1)}) all-reduce(f32[4]{0:T(128)S(1)} %dynamic-update-slice, f32[4]{0:T(128)S(1)} %fusion.165, f32[4]{0:T(128)S(1)} %dynamic-update-slice.3, f32[4]{0:T(128)S(1)} %dynamic-update-slice.6), channel_id=1, replica_groups=mesh['sp_0'=4,'sp_1'=4,'tp'=16] {'sp_1'}, use_global_device_ids=true, to_apply=%add | all-reduce | flops 16 | bytes 128
  60.8 2.6 fusion.161
  77.4 2.0 fusion.79
  87.9 9.3 %all-reduce.9 = (f32[4]{0:T(128)S(1)}, f32[4]{0:T(128)S(1)}, f32[4]{0:T(128)S(1)}, f32[4]{0:T(128)S(1)}) all-reduce(f32[4]{0:T(128)S(1)} %dynamic-update-slice.1, f32[4]{0:T(128)S(1)} %dynamic-update-slice.4, f32[4]{0:T(128)S(1)} %dynamic-update-slice.5, f32[4]{0:T(128)S(1)} %dynamic-update-slice.7), channel_id=2, replica_groups=mesh['sp_0'=4,'sp_1'=4,'tp'=16] {'sp_0'}, use_global_device_ids=true, to_apply=%add.1 | all-reduce | flops 16 | bytes 128
  126.2 9.6 %all-gather.8 = f32[4,1,256]{2,1,0:T(1,128)S(1)} all-gather(f32[1,1,256]{2,1,0:T(1,128)S(1)} %bitcast.323), channel_id=9, replica_groups=mesh['sp_0'=4,'sp_1'=4,'tp'=16] {'sp_1'}, dimensions={0}, use_global_device_ids=true | all-gather | bytes 5120 | tf_op jit(solution)/shard_map/all_gather | solution.py:25
  135.9 7.0 %all_gather.81 = f32[4,1,256]{2,1,0:T(1,128)S(1)} all-gather(f32[1,1,256]{2,1,0:T(1,128)S(1)} %get-tuple-element.176), channel_id=1, replica_groups=mesh['sp_0'=4,'sp_1'=4,'tp'=16] {'sp_0'}, dimensions={0}, use_global_device_ids=true | all-gather | bytes 5120 | tf_op jit(solution)/shard_map/all_gather | solution.py:25
  145.2 2.6 multiply_reduce_fusion.1
  147.8 2.2 convolution_convert_fusion.1
  150.6 60.0 %reduce-scatter.3.cloned.1.call-done = bf16[32,2048]{1,0:T(8,128)(2,1)} async-done(((bf16[512,2048]{1,0:T(8,128)(2,1)}), bf16[32,2048]{1,0:T(8,128)(2,1)}) %reduce-scatter.3.cloned.1.call-update) | async-done | bytes 131088 | tf_op jit(solution)/shard_map/reduce_scatter | solution.py:220
  213.4 15.8 %all_to_all.10 = bf16[16,5,2048]{2,1,0:T(8,128)(2,1)S(1)} all-to-all(bf16[16,5,2048]{2,1,0:T(8,128)(2,1)S(1)} %reshape.898), channel_id=1, replica_groups=mesh['sp_0'=4,'sp_1'=4,'tp'=16] {'sp_0','sp_1'}, dimensions={0} | all-to-all | bytes 655360 | tf_op jit(solution)/shard_map/all_to_all | solution.py:247
  229.4 7.7 %collective-permute-done = bf16[80,2048]{1,0:T(8,128)(2,1)S(1)} collective-permute-done((bf16[80,2048]{1,0:T(8,128)(2,1)S(1)}, bf16[80,2048]{1,0:T(8,128)(2,1)S(1)}, u32[]{:S(2)}, u32[]{:S(2)}) %collective-permute-start) | collective-permute-done | bytes 327712 | tf_op jit(solution)/shard_map/ppermute | solution.py:255
  237.1 3.0 collective-permute-start.8
  240.0 4.8 %collective-permute-done.1 = bf16[80,2048]{1,0:T(8,128)(2,1)S(1)} collective-permute-done((bf16[80,2048]{1,0:T(8,128)(2,1)S(1)}, bf16[80,2048]{1,0:T(8,128)(2,1)S(1)}, u32[]{:S(2)}, u32[]{:S(2)}) %collective-permute-start.1) | collective-permute-done | bytes 327712 | tf_op jit(solution)/shard_map/ppermute | solution.py:255
  244.8 3.0 collective-permute-start.9
  247.7 4.7 %collective-permute-done.2 = bf16[80,2048]{1,0:T(8,128)(2,1)S(1)} collective-permute-done((bf16[80,2048]{1,0:T(8,128)(2,1)S(1)}, bf16[80,2048]{1,0:T(8,128)(2,1)S(1)}, u32[]{:S(2)}, u32[]{:S(2)}) %collective-permute-start.2) | collective-permute-done | bytes 327712 | tf_op jit(solution)/shard_map/ppermute | solution.py:255
  252.5 3.0 collective-permute-start.10
  255.4 4.7 %collective-permute-done.3 = bf16[80,2048]{1,0:T(8,128)(2,1)S(1)} collective-permute-done((bf16[80,2048]{1,0:T(8,128)(2,1)S(1)}, bf16[80,2048]{1,0:T(8,128)(2,1)S(1)}, u32[]{:S(2)}, u32[]{:S(2)}) %collective-permute-start.3) | collective-permute-done | bytes 327712 | tf_op jit(solution)/shard_map/ppermute | solution.py:255
  260.2 3.0 collective-permute-start.11
  263.2 4.7 %collective-permute-done.4 = bf16[80,2048]{1,0:T(8,128)(2,1)S(1)} collective-permute-done((bf16[80,2048]{1,0:T(8,128)(2,1)S(1)}, bf16[80,2048]{1,0:T(8,128)(2,1)S(1)}, u32[]{:S(2)}, u32[]{:S(2)}) %collective-permute-start.4) | collective-permute-done | bytes 327712 | tf_op jit(solution)/shard_map/ppermute | solution.py:255
  268.7 2.9 collective-permute-start.12
  271.6 4.0 collective-permute-done.5
  276.2 3.2 collective-permute-start.13
  279.4 4.0 collective-permute-done.6
  284.3 3.1 collective-permute-start.14
  287.4 4.0 collective-permute-done.7
  304.2 4.0 copy-done.14
  308.1 2.6 fusion.52
  310.8 10.9 %convolution_convert_fusion = bf16[1280,2048]{1,0:T(8,128)(2,1)} fusion(bf16[1,256,2048]{2,1,0:T(8,128)(2,1)S(1)} %copy-done, f32[1280,256]{1,0:T(8,128)} %fusion.52, bf16[1,2048,256]{2,1,0:T(8,128)(2,1)} %param.30, bf16[2560,2048]{1,0:T(8,128)(2,1)} %copy-done.14, s32[]{:T(128)S(6)} %select_n.533), kind=kOutput, calls=%fused_computation.75 | convolution fusion | flops 2688942080 | bytes 13893636 | tf_op jit(solution)/shard_map/dot_general | solution.py:264
  322.4 61.4 %reduce-scatter.5.cloned.1.call-done = bf16[80,2048]{1,0:T(8,128)(2,1)} async-done(((bf16[1280,2048]{1,0:T(8,128)(2,1)}), bf16[80,2048]{1,0:T(8,128)(2,1)}) %reduce-scatter.5.cloned.1.call-update) | async-done | bytes 327696 | tf_op jit(solution)/shard_map/reduce_scatter | solution.py:263
  385.7 7.3 %all-to-all-start.1 = ((bf16[16,5,2048]{2,1,0:T(8,128)(2,1)}), bf16[16,5,2048]{2,1,0:T(8,128)(2,1)S(1)}, u32[]{:S(2)}, u32[]{:S(2)}) async-start(bf16[16,5,2048]{2,1,0:T(8,128)(2,1)} %reshape.900), calls=%async_computation.3 | async-start | bytes 1048576 | tf_op jit(solution)/shard_map/all_to_all | solution.py:270
  393.0 8.8 %all-to-all-done.1 = bf16[16,5,2048]{2,1,0:T(8,128)(2,1)S(1)} async-done(((bf16[16,5,2048]{2,1,0:T(8,128)(2,1)}), bf16[16,5,2048]{2,1,0:T(8,128)(2,1)S(1)}, u32[]{:S(2)}, u32[]{:S(2)}) %all-to-all-start.1) | async-done | bytes 327712 | tf_op jit(solution)/shard_map/all_to_all | solution.py:270
  (222 shorter events, 74.1 us)
Async XLA Ops:
  6.5 304.2 %copy-start = (bf16[1,256,2048]{2,1,0:T(8,128)(2,1)S(1)}, bf16[1,256,2048]{2,1,0:T(8,128)(2,1)}, u32[]{:S(2)}) copy-start(bf16[1,256,2048]{2,1,0:T(8,128)(2,1)} %param.31) | copy-start | bytes 3145732
  6.5 40.4 %copy-start.21 = (u32[256]{0:T(256)S(1)}, u32[256]{0:T(256)}, u32[]{:S(2)}) copy-start(u32[256]{0:T(256)} %constant.152) | copy-start | bytes 3076
  6.5 70.9 %all-gather.14.cloned.1.call-start = ((), (), s32[]{:S(2)}) async-start(), calls=%async_computation.7 | async-start | bytes 1310720 | tf_op jit(solution)/shard_map/all_gather | solution.py:25
  10.0 69.4 %copy-start.20 = (u32[256]{0:T(256)S(1)}, u32[256]{0:T(256)}, u32[]{:S(2)}) copy-start(u32[256]{0:T(256)} %constant.157) | copy-start | bytes 3076
  10.0 132.8 %copy-start.13 = (s32[512]{0:T(512)S(1)}, s32[512]{0:T(512)}, u32[]{:S(2)}) copy-start(s32[512]{0:T(512)} %param.23) | copy-start | bytes 6148
  10.1 137.7 %copy-start.12 = (bf16[256,2048]{1,0:T(8,128)(2,1)S(1)}, bf16[256,2048]{1,0:T(8,128)(2,1)}, u32[]{:S(2)}) copy-start(bf16[256,2048]{1,0:T(8,128)(2,1)} %param.25) | copy-start | bytes 3145732
  10.1 137.7 %copy-start.18 = (f32[256]{0:T(256)S(1)}, f32[256]{0:T(256)}, u32[]{:S(2)}) copy-start(f32[256]{0:T(256)} %param.24) | copy-start | bytes 3076
  40.6 109.5 %copy-start.15 = (s32[32,2]{0,1:T(2,128)S(1)}, s32[32,2]{0,1:T(2,128)}, u32[]{:S(2)}) copy-start(s32[32,2]{0,1:T(2,128)} %param.27) | copy-start | bytes 772
  40.6 170.0 %copy-start.10 = (bf16[32,2048]{1,0:T(8,128)(2,1)S(1)}, bf16[32,2048]{1,0:T(8,128)(2,1)}, u32[]{:S(2)}) copy-start(bf16[32,2048]{1,0:T(8,128)(2,1)} %param.17) | copy-start | bytes 393220
  40.6 171.1 %copy-start.16 = (f32[2048]{0:T(1024)S(1)}, f32[2048]{0:T(1024)}, u32[]{:S(2)}) copy-start(f32[2048]{0:T(1024)} %param.26) | copy-start | bytes 24580
  41.4 103.9 %all-gather.12.cloned.1.call-start = ((), (), s32[]{:S(2)}) async-start(), calls=%async_computation.4 | async-start | bytes 1310720 | tf_op jit(solution)/shard_map/all_gather | solution.py:25
  79.4 131.2 %reduce-scatter.3.cloned.1.call-start = ((), (), s32[]{:S(2)}) async-start(), calls=%async_computation.5 | async-start | bytes 2228224 | tf_op jit(solution)/shard_map/reduce_scatter | solution.py:220
  150.0 233.8 %reduce-scatter.5.cloned.1.call-start = ((), (), s32[]{:S(2)}) async-start(), calls=%async_computation.6 | async-start | bytes 5570560 | tf_op jit(solution)/shard_map/reduce_scatter | solution.py:263
  229.3 7.7 %collective-permute-start = (bf16[80,2048]{1,0:T(8,128)(2,1)S(1)}, bf16[80,2048]{1,0:T(8,128)(2,1)S(1)}, u32[]{:S(2)}, u32[]{:S(2)}) collective-permute-start(bf16[80,2048]{1,0:T(8,128)(2,1)S(1)} %reshape.899), channel_id=1, source_target_pairs={{0,1},{1,2},{2,3},{3,4},{4,5},{5,6},{6,7},{7,8},{8,9},{9,10},{10,1... | collective-permute-start | bytes 983048 | tf_op jit(solution)/shard_map/ppermute | solution.py:255
  237.1 7.7 %collective-permute-start.1 = (bf16[80,2048]{1,0:T(8,128)(2,1)S(1)}, bf16[80,2048]{1,0:T(8,128)(2,1)S(1)}, u32[]{:S(2)}, u32[]{:S(2)}) collective-permute-start(bf16[80,2048]{1,0:T(8,128)(2,1)S(1)} %collective-permute-done), channel_id=1, source_target_pairs={{0,1},{1,2},{2,3},{3,4},{4,5},{5,6},{6,7},{7,8},{8,9},{9,10},{10,1... | collective-permute-start | bytes 983048 | tf_op jit(solution)/shard_map/ppermute | solution.py:255
  237.1 7.7 %collective-permute-start.8 = (bf16[80,2048]{1,0:T(8,128)(2,1)S(1)}, bf16[80,2048]{1,0:T(8,128)(2,1)S(1)}, u32[]{:S(2)}, u32[]{:S(2)}) collective-permute-start(bf16[80,2048]{1,0:T(8,128)(2,1)S(1)} %reshape.899), channel_id=1, source_target_pairs={{0,15},{1,0},{2,1},{3,2},{4,3},{5,4},{6,5},{7,6},{8,7},{9,8},{10,9... | collective-permute-start | bytes 983048 | tf_op jit(solution)/shard_map/ppermute | solution.py:257
  244.8 7.7 %collective-permute-start.2 = (bf16[80,2048]{1,0:T(8,128)(2,1)S(1)}, bf16[80,2048]{1,0:T(8,128)(2,1)S(1)}, u32[]{:S(2)}, u32[]{:S(2)}) collective-permute-start(bf16[80,2048]{1,0:T(8,128)(2,1)S(1)} %collective-permute-done.1), channel_id=1, source_target_pairs={{0,1},{1,2},{2,3},{3,4},{4,5},{5,6},{6,7},{7,8},{8,9},{9,10},{10,1... | collective-permute-start | bytes 983048 | tf_op jit(solution)/shard_map/ppermute | solution.py:255
  244.8 7.7 %collective-permute-start.9 = (bf16[80,2048]{1,0:T(8,128)(2,1)S(1)}, bf16[80,2048]{1,0:T(8,128)(2,1)S(1)}, u32[]{:S(2)}, u32[]{:S(2)}) collective-permute-start(bf16[80,2048]{1,0:T(8,128)(2,1)S(1)} %collective-permute-done.8), channel_id=1, source_target_pairs={{0,15},{1,0},{2,1},{3,2},{4,3},{5,4},{6,5},{7,6},{8,7},{9,8},{10,9... | collective-permute-start | bytes 983048 | tf_op jit(solution)/shard_map/ppermute | solution.py:257
  252.5 7.7 %collective-permute-start.3 = (bf16[80,2048]{1,0:T(8,128)(2,1)S(1)}, bf16[80,2048]{1,0:T(8,128)(2,1)S(1)}, u32[]{:S(2)}, u32[]{:S(2)}) collective-permute-start(bf16[80,2048]{1,0:T(8,128)(2,1)S(1)} %collective-permute-done.2), channel_id=1, source_target_pairs={{0,1},{1,2},{2,3},{3,4},{4,5},{5,6},{6,7},{7,8},{8,9},{9,10},{10,1... | collective-permute-start | bytes 983048 | tf_op jit(solution)/shard_map/ppermute | solution.py:255
  252.5 7.7 %collective-permute-start.10 = (bf16[80,2048]{1,0:T(8,128)(2,1)S(1)}, bf16[80,2048]{1,0:T(8,128)(2,1)S(1)}, u32[]{:S(2)}, u32[]{:S(2)}) collective-permute-start(bf16[80,2048]{1,0:T(8,128)(2,1)S(1)} %collective-permute-done.9), channel_id=1, source_target_pairs={{0,15},{1,0},{2,1},{3,2},{4,3},{5,4},{6,5},{7,6},{8,7},{9,8},{10,9... | collective-permute-start | bytes 983048 | tf_op jit(solution)/shard_map/ppermute | solution.py:257
  260.2 7.7 %collective-permute-start.4 = (bf16[80,2048]{1,0:T(8,128)(2,1)S(1)}, bf16[80,2048]{1,0:T(8,128)(2,1)S(1)}, u32[]{:S(2)}, u32[]{:S(2)}) collective-permute-start(bf16[80,2048]{1,0:T(8,128)(2,1)S(1)} %collective-permute-done.3), channel_id=1, source_target_pairs={{0,1},{1,2},{2,3},{3,4},{4,5},{5,6},{6,7},{7,8},{8,9},{9,10},{10,1... | collective-permute-start | bytes 983048 | tf_op jit(solution)/shard_map/ppermute | solution.py:255
  260.2 7.7 %collective-permute-start.11 = (bf16[80,2048]{1,0:T(8,128)(2,1)S(1)}, bf16[80,2048]{1,0:T(8,128)(2,1)S(1)}, u32[]{:S(2)}, u32[]{:S(2)}) collective-permute-start(bf16[80,2048]{1,0:T(8,128)(2,1)S(1)} %collective-permute-done.10), channel_id=1, source_target_pairs={{0,15},{1,0},{2,1},{3,2},{4,3},{5,4},{6,5},{7,6},{8,7},{9,8},{10,9... | collective-permute-start | bytes 983048 | tf_op jit(solution)/shard_map/ppermute | solution.py:257
  267.9 7.7 %collective-permute-start.5 = (bf16[80,2048]{1,0:T(8,128)(2,1)S(1)}, bf16[80,2048]{1,0:T(8,128)(2,1)S(1)}, u32[]{:S(2)}, u32[]{:S(2)}) collective-permute-start(bf16[80,2048]{1,0:T(8,128)(2,1)S(1)} %collective-permute-done.4), channel_id=1, source_target_pairs={{0,1},{1,2},{2,3},{3,4},{4,5},{5,6},{6,7},{7,8},{8,9},{9,10},{10,1... | collective-permute-start | bytes 983048 | tf_op jit(solution)/shard_map/ppermute | solution.py:255
  268.7 7.5 %collective-permute-start.12 = (bf16[80,2048]{1,0:T(8,128)(2,1)S(1)}, bf16[80,2048]{1,0:T(8,128)(2,1)}, u32[]{:S(2)}, u32[]{:S(2)}) collective-permute-start(bf16[80,2048]{1,0:T(8,128)(2,1)S(1)} %collective-permute-done.11), channel_id=1, source_target_pairs={{0,15},{1,0},{2,1},{3,2},{4,3},{5,4},{6,5},{7,6},{8,7},{9,8},{10,9... | collective-permute-start | bytes 983048 | tf_op jit(solution)/shard_map/ppermute | solution.py:257
  275.6 7.8 %collective-permute-start.6 = (bf16[80,2048]{1,0:T(8,128)(2,1)S(1)}, bf16[80,2048]{1,0:T(8,128)(2,1)}, u32[]{:S(2)}, u32[]{:S(2)}) collective-permute-start(bf16[80,2048]{1,0:T(8,128)(2,1)S(1)} %collective-permute-done.5), channel_id=1, source_target_pairs={{0,1},{1,2},{2,3},{3,4},{4,5},{5,6},{6,7},{7,8},{8,9},{9,10},{10,1... | collective-permute-start | bytes 983048 | tf_op jit(solution)/shard_map/ppermute | solution.py:255
  276.2 8.1 %collective-permute-start.13 = (bf16[80,2048]{1,0:T(8,128)(2,1)}, bf16[80,2048]{1,0:T(8,128)(2,1)}, u32[]{:S(2)}, u32[]{:S(2)}) collective-permute-start(bf16[80,2048]{1,0:T(8,128)(2,1)} %collective-permute-done.12), channel_id=1, source_target_pairs={{0,15},{1,0},{2,1},{3,2},{4,3},{5,4},{6,5},{7,6},{8,7},{9,8},{10,9... | collective-permute-start | bytes 983048 | tf_op jit(solution)/shard_map/ppermute | solution.py:257
  283.4 8.0 %collective-permute-start.7 = (bf16[80,2048]{1,0:T(8,128)(2,1)}, bf16[80,2048]{1,0:T(8,128)(2,1)}, u32[]{:S(2)}, u32[]{:S(2)}) collective-permute-start(bf16[80,2048]{1,0:T(8,128)(2,1)} %collective-permute-done.6), channel_id=1, source_target_pairs={{0,1},{1,2},{2,3},{3,4},{4,5},{5,6},{6,7},{7,8},{8,9},{9,10},{10,1... | collective-permute-start | bytes 983048 | tf_op jit(solution)/shard_map/ppermute | solution.py:255
  283.5 18.6 %copy-start.3 = (bf16[80,2048]{1,0:T(8,128)(2,1)S(1)}, bf16[80,2048]{1,0:T(8,128)(2,1)}, u32[]{:S(2)}) copy-start(bf16[80,2048]{1,0:T(8,128)(2,1)} %copy-done.2) | copy-start | bytes 983044
  283.5 24.7 %copy-start.19 = (bf16[1,2048,256]{2,1,0:T(8,128)(2,1)S(1)}, bf16[1,2048,256]{2,1,0:T(8,128)(2,1)}, u32[]{:S(2)}) copy-start(bf16[1,2048,256]{2,1,0:T(8,128)(2,1)} %param.29) | copy-start | bytes 3145732
  284.3 15.4 %collective-permute-start.14 = (bf16[80,2048]{1,0:T(8,128)(2,1)}, bf16[80,2048]{1,0:T(8,128)(2,1)S(1)}, u32[]{:S(2)}, u32[]{:S(2)}) collective-permute-start(bf16[80,2048]{1,0:T(8,128)(2,1)} %collective-permute-done.13), channel_id=1, source_target_pairs={{0,15},{1,0},{2,1},{3,2},{4,3},{5,4},{6,5},{7,6},{8,7},{9,8},{10,9... | collective-permute-start | bytes 983048 | tf_op jit(solution)/shard_map/ppermute | solution.py:257
  321.7 82.8 %copy-start.11 = (bf16[32,2048]{1,0:T(8,128)(2,1)S(1)}, bf16[32,2048]{1,0:T(8,128)(2,1)}, u32[]{:S(2)}) copy-start(bf16[32,2048]{1,0:T(8,128)(2,1)} %reduce-scatter.3.cloned.1.call-done) | copy-start | bytes 393220
  385.7 16.0 %all-to-all-start.1 = ((bf16[16,5,2048]{2,1,0:T(8,128)(2,1)}), bf16[16,5,2048]{2,1,0:T(8,128)(2,1)S(1)}, u32[]{:S(2)}, u32[]{:S(2)}) async-start(bf16[16,5,2048]{2,1,0:T(8,128)(2,1)} %reshape.900), calls=%async_computation.3 | async-start | bytes 1048576 | tf_op jit(solution)/shard_map/all_to_all | solution.py:270
  (10 other events, 107.2 us)
Sparse Core Ops, SparseCore 0:
  41.5 28.4 all-gather.13
  79.5 28.0 all-gather.11
  150.1 60.4 reduce-scatter.2
  321.9 61.8 reduce-scatter.4
